TPU v7x, 32 devices: a whole 2x2x4 slice. The times are simulated.
32 devices in a mesh: sp: 16 (over z, y, x), dp: 2 (over core).
Axes of the slice: x: 2, y: 2, z: 4, core: 2. Of those that a mesh axis runs over, the one named last changes fastest.
Arguments:
- tokens: bfloat16 [2, 2048, 2048], P('dp', 'sp'), may hold values from -6 to 6
- w_value: bfloat16 [2048, 1024], P('dp', 'sp'), may hold values from -0.125 to 0.125
- w_gate: bfloat16 [2048, 1024], P('dp', 'sp'), may hold values from -0.125 to 0.125
- w_out: bfloat16 [1024, 2048], P('dp', 'sp'), may hold values from -0.1875 to 0.1875
- conv_taps: bfloat16 [1024, 31], replicated, may hold values from -1 to 1
- norm_gain: float32 [1024], replicated, may hold values from 0.1 to 1.9
- norm_bias: float32 [1024], replicated, may hold values from -3 to 3
Outputs:
- mixed: bfloat16 [2, 2048, 2048], P('dp', 'sp')
All inputs are finite; a program needn't handle non-finite values.
Results may differ from a plain program's by a relative error of at most 0.0064.
Values may be sent and summed in bfloat16 or wider, within the bound.
A program may use at most 64 MiB of HBM per device.

v0:
```python
import jax
import jax.numpy as jnp
from jax import lax
from jax.sharding import PartitionSpec as P


def padded_2(block, sides, width):
    for axis, dim in sides:
        count = lax.axis_size(axis)
        forward = [(i, i + 1) for i in range(count - 1)]
        backward = [(target, source) for source, target in forward]
        low = lax.ppermute(
            lax.slice_in_dim(block, block.shape[dim] - width, None, axis=dim), axis, forward
        )
        high = lax.ppermute(lax.slice_in_dim(block, 0, width, axis=dim), axis, backward)
        block = jnp.concatenate([low, block, high], axis=dim)
    return block


def depthwise(padded, taps, length):
    weights = taps.astype(jnp.float32)
    total = jnp.zeros((padded.shape[0], length), jnp.float32)
    for offset in range(taps.shape[1]):
        total = total + weights[:, offset : offset + 1] * padded[
            :, offset : offset + length
        ].astype(jnp.float32)
    return total.astype(jnp.bfloat16)


def normalize(conv_tok, norm_gain, norm_bias):
    values = lax.optimization_barrier(conv_tok).astype(jnp.float32)
    mean = jnp.mean(values, axis=0, keepdims=True)
    centred = values - mean
    variance = jnp.mean(centred * centred, axis=0, keepdims=True)
    normed = centred * lax.rsqrt(variance + 1e-05) * norm_gain[:, None] + norm_bias[:, None]
    return (normed * jax.nn.sigmoid(normed)).astype(jnp.bfloat16)


def on_device(tokens, w_value, w_gate, w_out, conv_taps, norm_gain, norm_bias):
    rows = tokens[0]
    contract_rows = (((0,), (1,)), ((), ()))
    contract_first = (((0,), (0,)), ((), ()))
    value_cols, gate_cols, out_cols = (
        lax.all_gather(w_value, "dp", axis=0, tiled=True),
        lax.all_gather(w_gate, "dp", axis=0, tiled=True),
        lax.all_gather(w_out, "dp", axis=0, tiled=True),
    )
    pieces = lax.all_gather((value_cols, gate_cols), "sp", axis=1, tiled=True)
    value = lax.dot_general(pieces[0], rows, contract_rows, preferred_element_type=jnp.float32)
    gate = lax.dot_general(pieces[1], rows, contract_rows, preferred_element_type=jnp.float32)
    gated_t = (value * jax.nn.sigmoid(gate)).astype(jnp.bfloat16)
    margin = conv_taps.shape[1] // 2
    padded = padded_2(gated_t, (("sp", 1),), margin)
    conv_tok = depthwise(padded, conv_taps, gated_t.shape[1])
    act_t = normalize(conv_tok, norm_gain, norm_bias)
    mixed = lax.dot_general(
        act_t,
        lax.all_gather(out_cols, "sp", axis=1, tiled=True),
        contract_first,
        preferred_element_type=jnp.float32,
    )
    return mixed.astype(jnp.bfloat16)[None]


def solution(mesh):
    in_specs = (P("dp", "sp", None), P("dp", "sp"), P("dp", "sp"), P("dp", "sp"), P(), P(), P())
    out_specs = P("dp", "sp", None)
    return jax.shard_map(
        on_device, mesh=mesh, in_specs=in_specs, out_specs=out_specs, check_vma=False
    )
```

profile of v0, /device:TPU:1, one launch (start us, length us, event | category | flops | bytes accessed | tf_op | source)
XLA Modules:
  0.0 264.8 jit_solution(798713640812950270)
XLA Ops:
  6.5 3.7 %all_gather.20 = bf16[2048,64]{0,1:T(8,128)(2,1)} all-gather(bf16[1024,64]{0,1:T(8,128)(2,1)} %param.9), channel_id=1, replica_groups=mesh['sp'=16,'dp'=2] {'dp'}, dimensions={0}, use_global_device_ids=true | all-gather | bytes 393216 | tf_op jit(solution)/shard_map/all_gather | solution.py:45
  10.2 0.0 all-gather.6.cloned.1.call-update
  10.2 0.0 all-gather.4.cloned.1.call-start
  10.3 3.8 %all_gather.18 = bf16[2048,64]{0,1:T(8,128)(2,1)} all-gather(bf16[1024,64]{0,1:T(8,128)(2,1)} %param.8), channel_id=1, replica_groups=mesh['sp'=16,'dp'=2] {'dp'}, dimensions={0}, use_global_device_ids=true | all-gather | bytes 393216 | tf_op jit(solution)/shard_map/all_gather | solution.py:44
  14.1 0.0 all-gather.4.cloned.1.call-update
  14.1 0.0 all-gather.8.cloned.1.call-start
  14.1 3.5 %all_gather.22 = bf16[1024,128]{1,0:T(8,128)(2,1)} all-gather(bf16[512,128]{1,0:T(8,128)(2,1)} %param.10), channel_id=1, replica_groups=mesh['sp'=16,'dp'=2] {'dp'}, dimensions={0}, use_global_device_ids=true | all-gather | bytes 393216 | tf_op jit(solution)/shard_map/all_gather | solution.py:46
  17.7 0.0 all-gather.8.cloned.1.call-update
  17.7 1.3 fusion.54
  19.0 67.5 %all-gather.6.cloned.1.call-done = bf16[2048,1024]{0,1:T(8,128)(2,1)} async-done(((bf16[2048,64]{0,1:T(8,128)(2,1)}), bf16[2048,1024]{0,1:T(8,128)(2,1)}) %all-gather.6.cloned.1.call-update) | async-done | bytes 4194320 | tf_op jit(solution)/shard_map/all_gather | solution.py:48
  86.4 3.7 %fusion.3 = f32[1024,128]{0,1:T(8,128)S(1)} fusion(bf16[2048,1024]{0,1:T(8,128)(2,1)} %all-gather.6.cloned.1.call-done, bf16[1,128,2048]{2,1,0:T(8,128)(2,1)S(1)} %copy-done), kind=kOutput, calls=%fused_computation.34 | convolution fusion | flops 537264128 | bytes 5242880 | tf_op jit(solution)/shard_map/dot_general | solution.py:50
  90.2 0.0 copy-start.1
  90.2 0.0 copy-start.2
  90.2 0.0 copy-start.3
  90.2 73.2 %all-gather.4.cloned.1.call-done = bf16[2048,1024]{0,1:T(8,128)(2,1)} async-done(((bf16[2048,64]{0,1:T(8,128)(2,1)}), bf16[2048,1024]{0,1:T(8,128)(2,1)}) %all-gather.4.cloned.1.call-update) | async-done | bytes 4194320 | tf_op jit(solution)/shard_map/all_gather | solution.py:48
  163.4 3.7 %fusion.4 = bf16[1024,128]{0,1:T(8,128)(2,1)S(1)} fusion(f32[1024,128]{0,1:T(8,128)S(1)} %fusion.3, bf16[2048,1024]{0,1:T(8,128)(2,1)} %all-gather.4.cloned.1.call-done, bf16[1,128,2048]{2,1,0:T(8,128)(2,1)S(1)} %copy-done), kind=kOutput, calls=%fused_computation.35 | convolution fusion | flops 537133056 | bytes 5505024 | tf_op jit(solution)/shard_map/dot_general | solution.py:49
  167.2 3.1 %collective-permute-start = (bf16[1024,15]{0,1:T(8,128)(2,1)S(1)}, bf16[1024,15]{0,1:T(8,128)(2,1)S(1)}, u32[]{:S(2)}, u32[]{:S(2)}) collective-permute-start(bf16[1024,15]{0,1:T(8,128)(2,1)S(1)} %get-tuple-element.5), channel_id=1, source_target_pairs={{0,2},{2,4},{4,6},{6,8},{8,10},{10,12},{12,14},{14,16},{16,18},{18... | collective-permute-start | bytes 92168 | tf_op jit(solution)/shard_map/ppermute | solution.py:12
  170.2 1.3 collective-permute-start.1
  171.6 3.3 %collective-permute-done.1 = bf16[1024,15]{0,1:T(8,128)(2,1)S(1)} collective-permute-done((bf16[1024,15]{0,1:T(8,128)(2,1)S(1)}, bf16[1024,15]{0,1:T(8,128)(2,1)S(1)}, u32[]{:S(2)}, u32[]{:S(2)}) %collective-permute-start.1) | collective-permute-done | bytes 30752 | tf_op jit(solution)/shard_map/ppermute | solution.py:15
  174.9 2.4 add_convert_fusion
  177.3 0.1 convert_reduce_fusion
  177.5 0.2 fusion.7
  177.7 76.7 %all-gather.8.cloned.1.call-done = bf16[1024,2048]{1,0:T(8,128)(2,1)} async-done(((bf16[1024,128]{1,0:T(8,128)(2,1)}), bf16[1024,2048]{1,0:T(8,128)(2,1)}) %all-gather.8.cloned.1.call-update) | async-done | bytes 4194320 | tf_op jit(solution)/shard_map/all_gather | solution.py:58
  254.4 3.9 %fusion = bf16[1,128,2048]{2,1,0:T(8,128)(2,1)} fusion(bf16[1024,2048]{1,0:T(8,128)(2,1)} %all-gather.8.cloned.1.call-done, bf16[1024,128]{0,1:T(8,128)(2,1)S(1)} %add_convert_fusion, f32[1024]{0:T(1024)S(1)} %copy-done.2, f32[1024]{0:T(1024)S(1)} %copy-done.3, f32[128]{0:T(128)S(1)} %add_rsqrt_fusion, f32[128]{0:T(128)S(1)} %broadcast_multiply_fusion), kind=kOutput, calls=%fused_computation.1 | convolution fusion | flops 538443776 | bytes 4989952 | tf_op jit(solution)/shard_map/dot_general | solution.py:56
  (11 shorter events, 0.1 us)
Async XLA Ops:
  6.5 79.9 %copy-start = (bf16[1,128,2048]{2,1,0:T(8,128)(2,1)S(1)}, bf16[1,128,2048]{2,1,0:T(8,128)(2,1)}, u32[]{:S(2)}) copy-start(bf16[1,128,2048]{2,1,0:T(8,128)(2,1)} %param.7) | copy-start | bytes 1572868
  6.5 79.9 %all-gather.6.cloned.1.call-start = ((), (), s32[]{:S(2)}) async-start(), calls=%async_computation.1 | async-start | bytes 4456448 | tf_op jit(solution)/shard_map/all_gather | solution.py:48
  10.2 153.2 %all-gather.4.cloned.1.call-start = ((), (), s32[]{:S(2)}) async-start(), calls=%async_computation | async-start | bytes 4456448 | tf_op jit(solution)/shard_map/all_gather | solution.py:48
  14.1 240.3 %all-gather.8.cloned.1.call-start = ((), (), s32[]{:S(2)}) async-start(), calls=%async_computation.2 | async-start | bytes 4456448 | tf_op jit(solution)/shard_map/all_gather | solution.py:58
  90.2 81.4 %copy-start.1 = (bf16[1024,31]{0,1:T(8,128)(2,1)S(1)}, bf16[1024,31]{0,1:T(8,128)(2,1)}, u32[]{:S(2)}) copy-start(bf16[1024,31]{0,1:T(8,128)(2,1)} %param.11) | copy-start | bytes 190468
  90.2 164.2 %copy-start.2 = (f32[1024]{0:T(1024)S(1)}, f32[1024]{0:T(1024)}, u32[]{:S(2)}) copy-start(f32[1024]{0:T(1024)} %param.13) | copy-start | bytes 12292
  90.2 164.2 %copy-start.3 = (f32[1024]{0:T(1024)S(1)}, f32[1024]{0:T(1024)}, u32[]{:S(2)}) copy-start(f32[1024]{0:T(1024)} %param.12) | copy-start | bytes 12292
  167.2 4.4 %collective-permute-start = (bf16[1024,15]{0,1:T(8,128)(2,1)S(1)}, bf16[1024,15]{0,1:T(8,128)(2,1)S(1)}, u32[]{:S(2)}, u32[]{:S(2)}) collective-permute-start(bf16[1024,15]{0,1:T(8,128)(2,1)S(1)} %get-tuple-element.5), channel_id=1, source_target_pairs={{0,2},{2,4},{4,6},{6,8},{8,10},{10,12},{12,14},{14,16},{16,18},{18... | collective-permute-start | bytes 92168 | tf_op jit(solution)/shard_map/ppermute | solution.py:12
  170.2 4.7 %collective-permute-start.1 = (bf16[1024,15]{0,1:T(8,128)(2,1)S(1)}, bf16[1024,15]{0,1:T(8,128)(2,1)S(1)}, u32[]{:S(2)}, u32[]{:S(2)}) collective-permute-start(bf16[1024,15]{0,1:T(8,128)(2,1)S(1)} %get-tuple-element.6), channel_id=1, source_target_pairs={{2,0},{4,2},{6,4},{8,6},{10,8},{12,10},{14,12},{16,14},{18,16},{20... | collective-permute-start | bytes 92168 | tf_op jit(solution)/shard_map/ppermute | solution.py:15
Sparse Core Ops, SparseCore 0:
  10.3 76.0 all-gather.5
  89.2 74.1 all-gather.3
  166.1 88.2 all-gather.7
where the time goes:
time: 267 us; the launch traced here: 265 us
  waiting for transfers between devices  221 us (83%)
  between operations  13.2 us (5%)
  matrix products  11.3 us (4%)
  blocking collectives  11 us (4%)
  starting transfers between devices  4.45 us (2%)
  other arithmetic  2.78 us (1%)
    all_gather x2, waiting for transfers between devices, on_device(): pieces = lax.all_gather((value_cols, gate_cols), 'sp', axis=1, tiled=True)  141 us
    all_gather x1, waiting for transfers between devices, on_device(): lax.all_gather(out_cols, 'sp', axis=1, tiled=True)  76.7 us
  transfers between devices with their start and end apart: 5, of which 4 were waited for; matrix products, arithmetic and copies ran while one was open for 4% of the time, Pallas kernels for 0%

commit v1 on v0

--- a/solution.py
+++ b/solution.py
@@ -1,7 +1,337 @@
+import functools
+
 import jax
 import jax.numpy as jnp
 from jax import lax
+from jax.experimental import pallas as pl
+from jax.experimental.pallas import tpu as pltpu
 from jax.sharding import PartitionSpec as P
+
+GROUP = 4
+LANES = 128
+EDGE = 16
+
+
+def kernel(depth_z, taps_count, tok_hbm, w_hbm, wo_hbm, taps_ref, gain_ref, bias_ref, out_ref,
+           tok, wg, wo, gp, cs, call, act,
+           load_sem, tok_s, tok_r, w_s, w_r, wd_s, wd_r, halo_s, halo_r,
+           cv_s, cv_r, oz_s, oz_r, op_s, op_r, od_s, od_r):
+    s, c = lax.axis_index("sp"), lax.axis_index("dp")
+    q, z = s % GROUP, s // GROUP
+    sx = s + 1 - 2 * (s % 2)
+    sy = s + 2 - 4 * ((s // 2) % 2)
+    sd = sx + 2 - 4 * ((sx // 2) % 2)
+    qx, qy, qd = sx % GROUP, sy % GROUP, sd % GROUP
+    rows, width = tok_hbm.shape
+    krows = w_hbm.shape[0]
+    orows, ocols = wo_hbm.shape
+    steps = depth_z - 1
+    span = GROUP * rows
+
+    def remote(src, dst, ss, rs, sp, dp):
+        return pltpu.make_async_remote_copy(
+            src_ref=src, dst_ref=dst, send_sem=ss, recv_sem=rs,
+            device_id={"sp": sp, "dp": dp}, device_id_type=pl.DeviceIdType.MESH)
+
+    def tok_at(who, half):
+        return tok.at[pl.ds(pl.multiple_of(who * rows + half * (rows // 2), rows // 2), rows // 2), :]
+
+    def wg_at(core, zz):
+        return wg.at[pl.ds(pl.multiple_of(core * krows, krows), krows),
+                     pl.ds(pl.multiple_of(zz * LANES, LANES), LANES)]
+
+    def wo_at(core, zz, who):
+        return wo.at[pl.ds(pl.multiple_of(core * orows, orows), orows),
+                     pl.ds(pl.multiple_of((zz * GROUP + who) * ocols, ocols), ocols)]
+
+    def wo_half(core, zz, who, half):
+        return wo.at[pl.ds(pl.multiple_of(core * orows + half * (orows // 2), orows // 2), orows // 2),
+                     pl.ds(pl.multiple_of((zz * GROUP + who) * ocols, ocols), ocols)]
+
+    def wo_plane(core, zz):
+        return wo.at[pl.ds(pl.multiple_of(core * orows, orows), orows),
+                     pl.ds(pl.multiple_of(zz * GROUP * ocols, GROUP * ocols), GROUP * ocols)]
+
+    loads = [
+        pltpu.make_async_copy(tok_hbm, tok.at[pl.ds(pl.multiple_of(q * rows, rows), rows), :], load_sem.at[0]),
+        pltpu.make_async_copy(w_hbm, wg_at(c, z), load_sem.at[1]),
+        pltpu.make_async_copy(wo_hbm, wo_at(c, z, q), load_sem.at[2]),
+    ]
+    for load in loads:
+        load.start()
+    barrier = pltpu.get_barrier_semaphore()
+
+    def greet(sp, dp):
+        pl.semaphore_signal(barrier, inc=1, device_id={"sp": sp, "dp": dp},
+                            device_id_type=pl.DeviceIdType.MESH)
+
+    for peer in (sx, sy, sd):
+        greet(peer, c)
+    greet(s, 1 - c)
+    pl.when(z > 0)(lambda: greet(s - GROUP, c))
+    pl.when(z < steps)(lambda: greet(s + GROUP, c))
+    ends = (z == 0).astype(jnp.int32) + (z == steps).astype(jnp.int32)
+    pl.semaphore_wait(barrier, 6 - ends)
+
+    slots = [(0, z, None)]
+    for step in range(steps):
+        slots.append((1 + step, z - 1 - step, z - 1 - step >= 0))
+        slots.append((1 + steps + step, z + 1 + step, z + 1 + step <= steps))
+    slots_by = {slot[0]: slot for slot in slots}
+
+    def guarded(cond, fn):
+        if cond is None:
+            fn()
+        else:
+            pl.when(cond)(fn)
+
+    def z_send(at, ss, rs, step):
+        up, down = z - step, z + step
+
+        def go_up():
+            remote(at(c, up), at(c, up), ss.at[0, step], rs.at[0, step], s + GROUP, c).start()
+
+        def go_down():
+            remote(at(c, down), at(c, down), ss.at[1, step], rs.at[1, step], s - GROUP, c).start()
+
+        pl.when((up >= 0) & (z < steps))(go_up)
+        pl.when((down <= steps) & (z > 0))(go_down)
+
+    def z_send_wait(at, ss, rs, step):
+        up, down = z - step, z + step
+        pl.when((up >= 0) & (z < steps))(
+            lambda: remote(at(c, up), at(c, up), ss.at[0, step], rs.at[0, step], s + GROUP, c).wait_send())
+        pl.when((down <= steps) & (z > 0))(
+            lambda: remote(at(c, down), at(c, down), ss.at[1, step], rs.at[1, step], s - GROUP, c).wait_send())
+
+    def z_recv(at, ss, rs, step):
+        lo, hi = z - 1 - step, z + 1 + step
+        pl.when(lo >= 0)(
+            lambda: remote(at(c, lo), at(c, lo), ss.at[0, step], rs.at[0, step], s - GROUP, c).wait_recv())
+        pl.when(hi <= steps)(
+            lambda: remote(at(c, hi), at(c, hi), ss.at[1, step], rs.at[1, step], s + GROUP, c).wait_recv())
+
+    def w_cross(slot):
+        index, zz, cond = slot
+        guarded(cond, lambda: remote(wg_at(c, zz), wg_at(c, zz), wd_s.at[index], wd_r.at[index], s, 1 - c).start())
+
+    def square_send(at, ss, rs):
+        for kind, half, peer in ((0, 0, sx), (2, 1, sy), (1, 1, sx), (3, 0, sy)):
+            remote(at(q, half), at(q, half), ss.at[kind], rs.at[kind], peer, c).start()
+
+    def square_pass(at, ss, rs):
+        remote(at(qx, 0), at(qx, 0), ss.at[0], rs.at[0], sx, c).wait_recv()
+        remote(at(qx, 0), at(qx, 0), ss.at[4], rs.at[4], sy, c).start()
+        remote(at(qy, 1), at(qy, 1), ss.at[2], rs.at[2], sy, c).wait_recv()
+        remote(at(qy, 1), at(qy, 1), ss.at[5], rs.at[5], sx, c).start()
+
+    def square_finish(at, ss, rs):
+        for kind, who, half, peer in ((1, qx, 1, sx), (3, qy, 0, sy), (4, qd, 0, sy), (5, qd, 1, sx)):
+            remote(at(who, half), at(who, half), ss.at[kind], rs.at[kind], peer, c).wait_recv()
+
+    def square_sent(at, ss, rs):
+        for kind, who, half, peer in ((0, q, 0, sx), (2, q, 1, sy), (1, q, 1, sx), (3, q, 0, sy),
+                                      (4, qx, 0, sy), (5, qy, 1, sx)):
+            remote(at(who, half), at(who, half), ss.at[kind], rs.at[kind], peer, c).wait_send()
+
+    def o_args(slot):
+        index, zz, cond = slot
+        return (functools.partial(wo_half, c, zz), op_s.at[index], op_r.at[index])
+
+    def own_wo(core, zz):
+        return wo_at(core, zz, q)
+
+    def o_cross(slot):
+        index, zz, cond = slot
+        return remote(wo_plane(c, zz), wo_plane(c, zz), od_s.at[index], od_r.at[index], s, 1 - c)
+
+    loads[0].wait()
+    square_send(tok_at, tok_s, tok_r)
+    loads[1].wait()
+    z_send(wg_at, w_s, w_r, 0)
+    w_cross(slots_by[0])
+    loads[2].wait()
+    for step in range(steps):
+        z_recv(wg_at, w_s, w_r, step)
+        if step + 1 < steps:
+            z_send(wg_at, w_s, w_r, step + 1)
+        w_cross(slots_by[1 + step])
+        w_cross(slots_by[1 + steps + step])
+        if step == 0:
+            square_pass(tok_at, tok_s, tok_r)
+            square_send(*o_args(slots_by[0]))
+        if step == steps - 2 or steps == 1:
+            z_send(own_wo, oz_s, oz_r, 0)
+    square_finish(tok_at, tok_s, tok_r)
+    for index, zz, cond in slots:
+        guarded(cond, lambda index=index, zz=zz: remote(
+            wg_at(1 - c, zz), wg_at(1 - c, zz), wd_s.at[index], wd_r.at[index], s, 1 - c).wait_recv())
+
+    tiles = depth_z // 2
+    lane = lax.broadcasted_iota(jnp.int32, (1, LANES), 1) < LANES // 2
+
+    def project(m, carry):
+        cols = pl.ds(pl.multiple_of(m * 2 * LANES, 2 * LANES), 2 * LANES)
+        both = jnp.dot(tok[...], wg[:, cols], preferred_element_type=jnp.float32)
+        first, second = both[:, :LANES], both[:, LANES:]
+        value = jnp.where(lane, first, pltpu.roll(second, LANES // 2, 1))
+        gate = jnp.where(lane, pltpu.roll(first, LANES // 2, 1), second)
+        gp[m, EDGE:EDGE + span, :] = (value * jax.nn.sigmoid(gate)).astype(jnp.bfloat16)
+        return carry
+
+    lax.fori_loop(0, tiles, project, 0)
+
+    low_edge, high_edge = gp.at[:, 0:EDGE, :], gp.at[:, EDGE + span:, :]
+    halo_up = lambda: remote(gp.at[:, span:EDGE + span, :], low_edge, halo_s.at[0], halo_r.at[0], s + GROUP, c)
+    halo_down = lambda: remote(gp.at[:, EDGE:2 * EDGE, :], high_edge, halo_s.at[1], halo_r.at[1], s - GROUP, c)
+    pl.when(z < steps)(lambda: halo_up().start())
+    pl.when(z > 0)(lambda: halo_down().start())
+
+    @pl.when(z == 0)
+    def _():
+        gp[:, 0:EDGE, :] = jnp.zeros((tiles, EDGE, LANES), gp.dtype)
+
+    @pl.when(z == steps)
+    def _():
+        gp[:, EDGE + span:, :] = jnp.zeros((tiles, EDGE, LANES), gp.dtype)
+
+    def o_arrive(step):
+        z_recv(own_wo, oz_s, oz_r, step)
+        if step + 1 < steps:
+            z_send(own_wo, oz_s, oz_r, step + 1)
+        for index in (1 + step, 1 + steps + step):
+            guarded(slots_by[index][2], lambda index=index: square_send(*o_args(slots_by[index])))
+
+    square_pass(*o_args(slots_by[0]))
+    o_arrive(0)
+    pl.when(z > 0)(lambda: halo_up().wait_recv())
+    pl.when(z < steps)(lambda: halo_down().wait_recv())
+
+    odd = (q % 2) == 1
+    chunk = 64
+
+    def convolve(i, carry):
+        m, r = i // (span // chunk), i % (span // chunk)
+        base = pl.multiple_of(m * 2 * GROUP * (LANES // 2) + (q // 2) * LANES, LANES)
+        near = taps_ref[:, pl.ds(base, LANES)]
+        far = taps_ref[:, pl.ds(pl.multiple_of(base + GROUP * (LANES // 2), LANES), LANES)]
+        taps = jnp.where(lane, jnp.where(odd, pltpu.roll(near, LANES // 2, 1), near),
+                         jnp.where(odd, far, pltpu.roll(far, LANES // 2, 1)))
+        x = gp[m, pl.ds(pl.multiple_of(r * chunk, chunk), chunk + 2 * EDGE), :].astype(jnp.float32)
+        total = jnp.zeros((chunk, LANES), jnp.float32)
+        shift = EDGE - taps_count // 2
+        for b in range(8):
+            moved = x[b:b + chunk + 24]
+            for a in range(4):
+                k = 8 * a + b - shift
+                if 0 <= k < taps_count:
+                    total = total + taps[k:k + 1] * moved[8 * a:8 * a + chunk]
+        cs[r // (rows // chunk), pl.ds(pl.multiple_of((r % (rows // chunk)) * chunk, chunk), chunk),
+           pl.ds(pl.multiple_of(m * LANES, LANES), LANES)] = total.astype(jnp.bfloat16)
+        return carry
+
+    lax.fori_loop(0, tiles * (span // chunk), convolve, 0)
+
+    sent = [remote(cs.at[who], call.at[q], cv_s.at[n], cv_r.at[n], peer, c)
+            for n, (who, peer) in enumerate(((qd, sd), (qx, sx), (qy, sy)))]
+    for copy in sent:
+        copy.start()
+    call[q] = cs[q]
+    for step in range(1, steps):
+        o_arrive(step)
+    for slot in slots[1:3]:
+        guarded(slot[2], lambda slot=slot: square_pass(*o_args(slot)))
+    square_finish(*o_args(slots[0]))
+    o_cross(slots[0]).start()
+    for n, (who, peer) in enumerate(((qd, sd), (qx, sx), (qy, sy))):
+        remote(cs.at[who], call.at[who], cv_s.at[n], cv_r.at[n], peer, c).wait_recv()
+
+    channels = gain_ref.shape[1]
+    pieces = []
+    for t in range(channels // LANES):
+        zz, pair = t // 2, 2 * (t % 2)
+        a = call[pair, :, (zz // 2) * LANES:(zz // 2 + 1) * LANES].astype(jnp.float32)
+        b = call[pair + 1, :, (zz // 2) * LANES:(zz // 2 + 1) * LANES].astype(jnp.float32)
+        if zz % 2 == 0:
+            pieces.append(jnp.where(lane, a, pltpu.roll(b, LANES // 2, 1)))
+        else:
+            pieces.append(jnp.where(lane, pltpu.roll(a, LANES // 2, 1), b))
+    conv = jnp.concatenate(pieces, axis=1)
+    mean = jnp.sum(conv, axis=1, keepdims=True) * (1.0 / channels)
+    centred = conv - mean
+    variance = jnp.sum(centred * centred, axis=1, keepdims=True) * (1.0 / channels)
+    normed = centred * lax.rsqrt(variance + 1e-05) * gain_ref[...] + bias_ref[...]
+    act[...] = (normed * jax.nn.sigmoid(normed)).astype(jnp.bfloat16)
+
+    def finish(slot):
+        index, zz, cond = slot
+        remote(wo_plane(1 - c, zz), wo_plane(1 - c, zz), od_s.at[index], od_r.at[index], s, 1 - c).wait_recv()
+        cols = pl.ds(pl.multiple_of(zz * GROUP * ocols, GROUP * ocols), GROUP * ocols)
+        out_ref[:, cols] = jnp.dot(act[...], wo[:, cols], preferred_element_type=jnp.float32).astype(jnp.bfloat16)
+
+    def gather(slot):
+        square_finish(*o_args(slot))
+        o_cross(slot).start()
+
+    for n, slot in enumerate(slots):
+        for later in slots[2 * n + 3:2 * n + 5] if n < steps else ():
+            guarded(later[2], lambda later=later: square_pass(*o_args(later)))
+        if n > 0:
+            guarded(slot[2], lambda slot=slot: gather(slot))
+    for slot in slots:
+        guarded(slot[2], lambda slot=slot: finish(slot))
+
+    square_sent(tok_at, tok_s, tok_r)
+    for step in range(steps):
+        z_send_wait(wg_at, w_s, w_r, step)
+        z_send_wait(own_wo, oz_s, oz_r, step)
+    pl.when(z < steps)(lambda: halo_up().wait_send())
+    pl.when(z > 0)(lambda: halo_down().wait_send())
+    for copy in sent:
+        copy.wait_send()
+    for slot in slots:
+        def drain(slot=slot):
+            index, zz, cond = slot
+            remote(wg_at(c, zz), wg_at(c, zz), wd_s.at[index], wd_r.at[index], s, 1 - c).wait_send()
+            square_sent(*o_args(slot))
+            o_cross(slot).wait_send()
+        guarded(slot[2], drain)
+
+
+def fused(depth_z, tokens, w_value, w_gate, w_out, conv_taps, norm_gain, norm_bias):
+    rows, width = tokens.shape[1:]
+    krows = w_value.shape[0]
+    orows, ocols = w_out.shape
+    channels, taps_count = conv_taps.shape
+    pair = jnp.concatenate([w_value, w_gate], axis=1)
+    taps = jnp.pad(conv_taps.astype(jnp.float32).T, ((0, 2 * EDGE - taps_count), (0, 0)))
+    steps, tiles, span = depth_z - 1, depth_z // 2, GROUP * rows
+    slots = 1 + 2 * steps
+    dma = pltpu.SemaphoreType.DMA
+    near = pl.BlockSpec(memory_space=pltpu.VMEM)
+    far = pl.BlockSpec(memory_space=pl.ANY)
+    bf16 = jnp.bfloat16
+    mixed = pl.pallas_call(
+        functools.partial(kernel, depth_z, taps_count),
+        out_shape=jax.ShapeDtypeStruct((rows, w_out.shape[1] * GROUP * depth_z), bf16),
+        in_specs=[far, far, far, near, near, near],
+        out_specs=near,
+        scratch_shapes=[
+            pltpu.VMEM((span, width), bf16),
+            pltpu.VMEM((2 * krows, depth_z * LANES), bf16),
+            pltpu.VMEM((2 * orows, depth_z * GROUP * ocols), bf16),
+            pltpu.VMEM((tiles, span + 2 * EDGE, LANES), bf16),
+            pltpu.VMEM((GROUP, rows, tiles * LANES), bf16),
+            pltpu.VMEM((GROUP, rows, tiles * LANES), bf16),
+            pltpu.VMEM((rows, channels), bf16),
+            dma((3,)), dma((6,)), dma((6,)), dma((2, steps)), dma((2, steps)),
+            dma((slots,)), dma((slots,)), dma((2,)), dma((2,)),
+            dma((3,)), dma((3,)), dma((2, steps)), dma((2, steps)),
+            dma((slots, 6)), dma((slots, 6)), dma((slots,)), dma((slots,)),
+        ],
+        compiler_params=pltpu.CompilerParams(collective_id=0, has_side_effects=True),
+    )(tokens[0], pair, w_out, taps, norm_gain[None], norm_bias[None])
+    return mixed[None]
 
 
 def padded_2(block, sides, width):
@@ -62,9 +392,19 @@
     return mixed.astype(jnp.bfloat16)[None]
 
 
+def on_any(tokens, w_value, w_gate, w_out, conv_taps, norm_gain, norm_bias):
+    count, cores = lax.axis_size("sp"), lax.axis_size("dp")
+    depth_z = count // GROUP
+    fits = (cores == 2 and count % (2 * GROUP) == 0 and tokens.shape[0] == 1
+            and 2 * w_value.shape[1] == LANES and w_out.shape[1] % LANES == 0
+            and tokens.shape[1] % LANES == 0 and conv_taps.shape[1] // 2 < EDGE)
+    args = (tokens, w_value, w_gate, w_out, conv_taps, norm_gain, norm_bias)
+    return fused(depth_z, *args) if fits else on_device(*args)
+
+
 def solution(mesh):
     in_specs = (P("dp", "sp", None), P("dp", "sp"), P("dp", "sp"), P("dp", "sp"), P(), P(), P())
     out_specs = P("dp", "sp", None)
     return jax.shard_map(
-        on_device, mesh=mesh, in_specs=in_specs, out_specs=out_specs, check_vma=False
+        on_any, mesh=mesh, in_specs=in_specs, out_specs=out_specs, check_vma=False
     )

time: 267 us -> 59.2 us (0.22)
  waiting for transfers between devices: 221 us -> 0 us
  Pallas kernels: 0 us -> 53.6 us
  between operations: 13.2 us -> 0.02 us
  matrix products: 11.3 us -> 0 us
  blocking collectives: 11 us -> 0 us
  starting transfers between devices: 4.45 us -> 0 us
    all_gather x3 -> x0, waiting for transfers between devices: 217 us -> none  [the longest x2 141 us: on_device(): pieces = lax.all_gather((value_cols, gate_cols), 'sp', axis=1, tiled=True)]
    pallas_call x0 -> x1, Pallas kernels: none -> 53.6 us  [fused(): pl.pallas_call(functools.partial(kernel, depth_z, taps_count), out_shape=...]
    dot_general x3 -> x0, matrix products: 11.3 us -> none  [the longest x1 3.87 us: on_device(): lax.dot_general(act_t, lax.all_gather(out_cols, 'sp', axis=1, tiled=True)...]
    all_gather x3 -> x0, blocking collectives: 11 us -> none  [the longest x1 3.77 us: on_device(): lax.all_gather(w_value, 'dp', axis=0, tiled=True)]
    ppermute x2 -> x0, starting transfers between devices: 4.36 us -> none  [the longest x1 3.07 us: padded_2(): lax.ppermute(lax.slice_in_dim(block, block.shape[dim] - width, None, axis...]
    ppermute x2 -> x0, waiting for transfers between devices: 3.29 us -> none  [the longest x1 3.29 us: padded_2(): lax.ppermute(lax.slice_in_dim(block, 0, width, axis=dim), axis, backward)]
    unnamed x8 -> x7, local copies, waits for them, and re-layouts: 0.02 us -> 2.95 us
  transfers between devices with their start and end apart: 5 -> 0, of which waited for: 4 -> 0; matrix products, arithmetic and copies ran while one was open for 4% -> 0% of each run, Pallas kernels for 0% -> 0%
where the time goes in v1:
time: 59.2 us; the launch traced here: 59 us
  Pallas kernels  53.6 us (91%)
  local copies, waits for them, and re-layouts  2.95 us (5%)
  other arithmetic  2.39 us (4%)
    pallas_call x1, Pallas kernels, fused(): pl.pallas_call(functools.partial(kernel, depth_z, taps_count), out_shape=...  53.6 us
    unnamed x7, local copies, waits for them, and re-layouts  2.95 us
    pad x1, other arithmetic, fused(): jnp.pad(conv_taps.astype(jnp.float32).T, ((0, 2 * EDGE - taps_count), (0,...  1.54 us

profile of v1, /device:TPU:1, one launch (start us, length us, event | category | flops | bytes accessed | tf_op | source)
XLA Modules:
  0.0 59.0 jit_solution(11051858547011735636)
XLA Ops:
  0.0 0.0 copy-start
  0.0 1.5 %pad_convert_fusion.taps_ref = f32[32,1024]{1,0:T(8,128)} fusion(bf16[31,1024]{1,0:T(8,128)(2,1)} %bitcast.7), kind=kLoop, calls=%fused_computation.1 | loop fusion | flops 32768 | bytes 194560 | tf_op jit(solution)/shard_map/jit(_pad)/pad | solution.py:307
  1.5 0.0 copy-done
  1.5 0.0 copy-start.1
  1.5 0.2 copy.8
  1.7 0.7 %copy-done.1 = bf16[1024,64]{0,1:T(8,128)(2,1)S(1)} copy-done((bf16[1024,64]{0,1:T(8,128)(2,1)S(1)}, bf16[1024,64]{0,1:T(8,128)(2,1)}, u32[]{:S(2)}) %copy-start.1) | copy-done | bytes 131096
  2.4 0.2 copy.9
  2.6 0.9 %pad_maximum_fusion.w_hbm = bf16[1024,128]{1,0:T(8,128)(2,1)} fusion(bf16[1024,64]{1,0:T(8,128)(2,1)S(1)} %copy.9, bf16[1024,64]{1,0:T(8,128)(2,1)S(1)} %copy.8), kind=kLoop, calls=%fused_computation | loop fusion | flops 524288 | bytes 524288 | tf_op jit(solution)/shard_map/concatenate | solution.py:306
  3.5 53.6 %shard_map.73 = bf16[128,2048]{1,0:T(8,128)(2,1)} custom-call(bf16[128,2048]{1,0:T(8,128)(2,1)} %bitcast.6, bf16[1024,128]{1,0:T(8,128)(2,1)} %pad_maximum_fusion.w_hbm, bf16[512,128]{1,0:T(8,128)(2,1)} %wo_hbm.1, f32[32,1024]{1,0:T(8,128)} %pad_convert_fusion.taps_ref, f32[1,1024]{1,0:T(1,128)} %bitcast.8, f32[1,1024]{1,0:T(1,128)} %bitcast.9), custom_call_target="tpu_custom_call" | custom-call | tf_op jit(solution)/shard_map/pallas_call | solution.py:314
  57.1 1.9 %copy.11 = bf16[1,128,2048]{2,1,0:T(8,128)(2,1)} copy(bf16[1,128,2048]{2,1,0:T(8,128)(2,1)} %bitcast.5) | data formatting | bytes 1048576
Async XLA Ops:
  0.0 1.5 %copy-start = (bf16[1024,64]{0,1:T(8,128)(2,1)S(1)}, bf16[1024,64]{0,1:T(8,128)(2,1)}, u32[]{:S(2)}) copy-start(bf16[1024,64]{0,1:T(8,128)(2,1)} %param.8) | copy-start | bytes 393220
  1.5 0.9 %copy-start.1 = (bf16[1024,64]{0,1:T(8,128)(2,1)S(1)}, bf16[1024,64]{0,1:T(8,128)(2,1)}, u32[]{:S(2)}) copy-start(bf16[1024,64]{0,1:T(8,128)(2,1)} %param.9) | copy-start | bytes 393220

commit v2 on v1

--- a/solution.py
+++ b/solution.py
@@ -12,8 +12,8 @@
 EDGE = 16
 
 
-def kernel(depth_z, taps_count, tok_hbm, w_hbm, wo_hbm, taps_ref, gain_ref, bias_ref, out_ref,
-           tok, wg, wo, gp, cs, call, act,
+def kernel(depth_z, taps_count, tok_hbm, wv_hbm, wg_hbm, wo_hbm, taps_ref, gain_ref, bias_ref, out_ref,
+           tok, wg, wo, gp, cs, call, act, tb,
            load_sem, tok_s, tok_r, w_s, w_r, wd_s, wd_r, halo_s, halo_r,
            cv_s, cv_r, oz_s, oz_r, op_s, op_r, od_s, od_r):
     s, c = lax.axis_index("sp"), lax.axis_index("dp")
@@ -23,7 +23,7 @@
     sd = sx + 2 - 4 * ((sx // 2) % 2)
     qx, qy, qd = sx % GROUP, sy % GROUP, sd % GROUP
     rows, width = tok_hbm.shape
-    krows = w_hbm.shape[0]
+    wcols, krows = wv_hbm.shape
     orows, ocols = wo_hbm.shape
     steps = depth_z - 1
     span = GROUP * rows
@@ -37,8 +37,8 @@
         return tok.at[pl.ds(pl.multiple_of(who * rows + half * (rows // 2), rows // 2), rows // 2), :]
 
     def wg_at(core, zz):
-        return wg.at[pl.ds(pl.multiple_of(core * krows, krows), krows),
-                     pl.ds(pl.multiple_of(zz * LANES, LANES), LANES)]
+        return wg.at[:, pl.ds(pl.multiple_of(zz * wcols, wcols), wcols),
+                     pl.ds(pl.multiple_of(core * krows, krows), krows)]
 
     def wo_at(core, zz, who):
         return wo.at[pl.ds(pl.multiple_of(core * orows, orows), orows),
@@ -54,7 +54,8 @@
 
     loads = [
         pltpu.make_async_copy(tok_hbm, tok.at[pl.ds(pl.multiple_of(q * rows, rows), rows), :], load_sem.at[0]),
-        pltpu.make_async_copy(w_hbm, wg_at(c, z), load_sem.at[1]),
+        pltpu.make_async_copy(wv_hbm, wg_at(c, z).at[0], load_sem.at[1]),
+        pltpu.make_async_copy(wg_hbm, wg_at(c, z).at[1], load_sem.at[3]),
         pltpu.make_async_copy(wo_hbm, wo_at(c, z, q), load_sem.at[2]),
     ]
     for load in loads:
@@ -148,9 +149,21 @@
     loads[0].wait()
     square_send(tok_at, tok_s, tok_r)
     loads[1].wait()
+    loads[2].wait()
     z_send(wg_at, w_s, w_r, 0)
     w_cross(slots_by[0])
-    loads[2].wait()
+    loads[3].wait()
+    tiles = depth_z // 2
+    lane = lax.broadcasted_iota(jnp.int32, (1, LANES), 1) < LANES // 2
+    odd = (q % 2) == 1
+    for m in range(tiles):
+        base = pl.multiple_of(m * GROUP * LANES + (q // 2) * LANES, LANES)
+        near = taps_ref[:, pl.ds(base, LANES)].astype(jnp.float32)
+        far = taps_ref[:, pl.ds(pl.multiple_of(base + GROUP // 2 * LANES, LANES), LANES)].astype(jnp.float32)
+        taps = jnp.where(lane, jnp.where(odd, pltpu.roll(near, LANES // 2, 1), near),
+                         jnp.where(odd, far, pltpu.roll(far, LANES // 2, 1)))
+        for k in range(taps_count):
+            tb[m, k] = jnp.broadcast_to(taps[k:k + 1], (8, LANES))
     for step in range(steps):
         z_recv(wg_at, w_s, w_r, step)
         if step + 1 < steps:
@@ -162,20 +175,31 @@
             square_send(*o_args(slots_by[0]))
         if step == steps - 2 or steps == 1:
             z_send(own_wo, oz_s, oz_r, 0)
+    def o_line(step):
+        z_recv(own_wo, oz_s, oz_r, step)
+        if step + 1 < steps:
+            z_send(own_wo, oz_s, oz_r, step + 1)
+        each(step, lambda slot: square_send(*o_args(slot)))
+
+    def each(step, fn):
+        for index in (1 + step, 1 + steps + step):
+            slot = slots_by[index]
+            guarded(slot[2], lambda slot=slot: fn(slot))
+
+    def o_pass(slot):
+        square_pass(*o_args(slot))
+
+    o_line(0)
     square_finish(tok_at, tok_s, tok_r)
     for index, zz, cond in slots:
         guarded(cond, lambda index=index, zz=zz: remote(
             wg_at(1 - c, zz), wg_at(1 - c, zz), wd_s.at[index], wd_r.at[index], s, 1 - c).wait_recv())
 
-    tiles = depth_z // 2
-    lane = lax.broadcasted_iota(jnp.int32, (1, LANES), 1) < LANES // 2
-
     def project(m, carry):
-        cols = pl.ds(pl.multiple_of(m * 2 * LANES, 2 * LANES), 2 * LANES)
-        both = jnp.dot(tok[...], wg[:, cols], preferred_element_type=jnp.float32)
-        first, second = both[:, :LANES], both[:, LANES:]
-        value = jnp.where(lane, first, pltpu.roll(second, LANES // 2, 1))
-        gate = jnp.where(lane, pltpu.roll(first, LANES // 2, 1), second)
+        cols = pl.ds(pl.multiple_of(m * LANES, LANES), LANES)
+        across = (((1,), (1,)), ((), ()))
+        value = lax.dot_general(tok[...], wg[0, cols, :], across, preferred_element_type=jnp.float32)
+        gate = lax.dot_general(tok[...], wg[1, cols, :], across, preferred_element_type=jnp.float32)
         gp[m, EDGE:EDGE + span, :] = (value * jax.nn.sigmoid(gate)).astype(jnp.bfloat16)
         return carry
 
@@ -195,52 +219,44 @@
     def _():
         gp[:, EDGE + span:, :] = jnp.zeros((tiles, EDGE, LANES), gp.dtype)
 
-    def o_arrive(step):
-        z_recv(own_wo, oz_s, oz_r, step)
-        if step + 1 < steps:
-            z_send(own_wo, oz_s, oz_r, step + 1)
-        for index in (1 + step, 1 + steps + step):
-            guarded(slots_by[index][2], lambda index=index: square_send(*o_args(slots_by[index])))
-
-    square_pass(*o_args(slots_by[0]))
-    o_arrive(0)
-    pl.when(z > 0)(lambda: halo_up().wait_recv())
-    pl.when(z < steps)(lambda: halo_down().wait_recv())
-
-    odd = (q % 2) == 1
     chunk = 64
-
-    def convolve(i, carry):
-        m, r = i // (span // chunk), i % (span // chunk)
-        base = pl.multiple_of(m * 2 * GROUP * (LANES // 2) + (q // 2) * LANES, LANES)
-        near = taps_ref[:, pl.ds(base, LANES)]
-        far = taps_ref[:, pl.ds(pl.multiple_of(base + GROUP * (LANES // 2), LANES), LANES)]
-        taps = jnp.where(lane, jnp.where(odd, pltpu.roll(near, LANES // 2, 1), near),
-                         jnp.where(odd, far, pltpu.roll(far, LANES // 2, 1)))
+    chunks = span // chunk
+
+    def convolve(m, r):
         x = gp[m, pl.ds(pl.multiple_of(r * chunk, chunk), chunk + 2 * EDGE), :].astype(jnp.float32)
-        total = jnp.zeros((chunk, LANES), jnp.float32)
+        total = jnp.zeros((chunk // 8, 8, LANES), jnp.float32)
         shift = EDGE - taps_count // 2
         for b in range(8):
-            moved = x[b:b + chunk + 24]
+            moved = x[b:b + chunk + 24].reshape(chunk // 8 + 3, 8, LANES)
             for a in range(4):
                 k = 8 * a + b - shift
                 if 0 <= k < taps_count:
-                    total = total + taps[k:k + 1] * moved[8 * a:8 * a + chunk]
+                    total = total + tb[m, k][None] * moved[a:a + chunk // 8]
         cs[r // (rows // chunk), pl.ds(pl.multiple_of((r % (rows // chunk)) * chunk, chunk), chunk),
-           pl.ds(pl.multiple_of(m * LANES, LANES), LANES)] = total.astype(jnp.bfloat16)
+           pl.ds(pl.multiple_of(m * LANES, LANES), LANES)] = total.reshape(chunk, LANES).astype(jnp.bfloat16)
+
+    def inner(i, carry):
+        convolve(i // (chunks - 2), i % (chunks - 2) + 1)
         return carry
 
-    lax.fori_loop(0, tiles * (span // chunk), convolve, 0)
+    def outer(i, carry):
+        convolve(i // 2, (i % 2) * (chunks - 1))
+        return carry
+
+    o_pass(slots[0])
+    lax.fori_loop(0, tiles * (chunks - 2), inner, 0)
+    pl.when(z > 0)(lambda: halo_up().wait_recv())
+    pl.when(z < steps)(lambda: halo_down().wait_recv())
+    lax.fori_loop(0, tiles * 2, outer, 0)
 
     sent = [remote(cs.at[who], call.at[q], cv_s.at[n], cv_r.at[n], peer, c)
             for n, (who, peer) in enumerate(((qd, sd), (qx, sx), (qy, sy)))]
     for copy in sent:
         copy.start()
     call[q] = cs[q]
+    each(0, o_pass)
     for step in range(1, steps):
-        o_arrive(step)
-    for slot in slots[1:3]:
-        guarded(slot[2], lambda slot=slot: square_pass(*o_args(slot)))
+        o_line(step)
     square_finish(*o_args(slots[0]))
     o_cross(slots[0]).start()
     for n, (who, peer) in enumerate(((qd, sd), (qx, sx), (qy, sy))):
@@ -273,13 +289,14 @@
         square_finish(*o_args(slot))
         o_cross(slot).start()
 
-    for n, slot in enumerate(slots):
-        for later in slots[2 * n + 3:2 * n + 5] if n < steps else ():
-            guarded(later[2], lambda later=later: square_pass(*o_args(later)))
-        if n > 0:
-            guarded(slot[2], lambda slot=slot: gather(slot))
-    for slot in slots:
-        guarded(slot[2], lambda slot=slot: finish(slot))
+    finish(slots[0])
+    for step in range(steps):
+        if step + 1 < steps:
+            each(step + 1, o_pass)
+        each(step, gather)
+        if step > 0:
+            each(step - 1, finish)
+    each(steps - 1, finish)
 
     square_sent(tok_at, tok_s, tok_r)
     for step in range(steps):
@@ -303,8 +320,6 @@
     krows = w_value.shape[0]
     orows, ocols = w_out.shape
     channels, taps_count = conv_taps.shape
-    pair = jnp.concatenate([w_value, w_gate], axis=1)
-    taps = jnp.pad(conv_taps.astype(jnp.float32).T, ((0, 2 * EDGE - taps_count), (0, 0)))
     steps, tiles, span = depth_z - 1, depth_z // 2, GROUP * rows
     slots = 1 + 2 * steps
     dma = pltpu.SemaphoreType.DMA
@@ -313,24 +328,25 @@
     bf16 = jnp.bfloat16
     mixed = pl.pallas_call(
         functools.partial(kernel, depth_z, taps_count),
-        out_shape=jax.ShapeDtypeStruct((rows, w_out.shape[1] * GROUP * depth_z), bf16),
-        in_specs=[far, far, far, near, near, near],
+        out_shape=pltpu.VMEM((rows, w_out.shape[1] * GROUP * depth_z), bf16),
+        in_specs=[far, far, far, far, near, near, near],
         out_specs=near,
         scratch_shapes=[
             pltpu.VMEM((span, width), bf16),
-            pltpu.VMEM((2 * krows, depth_z * LANES), bf16),
+            pltpu.VMEM((2, depth_z * w_value.shape[1], 2 * krows), bf16),
             pltpu.VMEM((2 * orows, depth_z * GROUP * ocols), bf16),
             pltpu.VMEM((tiles, span + 2 * EDGE, LANES), bf16),
             pltpu.VMEM((GROUP, rows, tiles * LANES), bf16),
             pltpu.VMEM((GROUP, rows, tiles * LANES), bf16),
             pltpu.VMEM((rows, channels), bf16),
-            dma((3,)), dma((6,)), dma((6,)), dma((2, steps)), dma((2, steps)),
+            pltpu.VMEM((tiles, taps_count, 8, LANES), jnp.float32),
+            dma((4,)), dma((6,)), dma((6,)), dma((2, steps)), dma((2, steps)),
             dma((slots,)), dma((slots,)), dma((2,)), dma((2,)),
             dma((3,)), dma((3,)), dma((2, steps)), dma((2, steps)),
             dma((slots, 6)), dma((slots, 6)), dma((slots,)), dma((slots,)),
         ],
         compiler_params=pltpu.CompilerParams(collective_id=0, has_side_effects=True),
-    )(tokens[0], pair, w_out, taps, norm_gain[None], norm_bias[None])
+    )(tokens[0], w_value.T, w_gate.T, w_out, conv_taps.T, norm_gain[None], norm_bias[None])
     return mixed[None]
 
 

time: 59.2 us -> 53.6 us (0.905)
  other arithmetic: 2.39 us -> 0 us
  local copies, waits for them, and re-layouts: 2.95 us -> 0.8 us
  Pallas kernels: 53.6 us -> 52.6 us
    unnamed x7 -> x1, local copies, waits for them, and re-layouts: 2.95 us -> 0.8 us
    pad x1 -> x0, other arithmetic: 1.54 us -> none  [fused(): jnp.pad(conv_taps.astype(jnp.float32).T, ((0, 2 * EDGE - taps_count), (0,...]
    pallas_call x1, Pallas kernels: 53.6 us -> 52.6 us  [fused(): pl.pallas_call(functools.partial(kernel, depth_z, taps_count), out_shape=...]
    concatenate x1 -> x0, other arithmetic: 0.86 us -> none  [fused(): pair = jnp.concatenate([w_value, w_gate], axis=1)]
where the time goes in v2:
time: 53.6 us; the launch traced here: 53.4 us
  Pallas kernels  52.6 us (98%)
  local copies, waits for them, and re-layouts  0.8 us (1%)
    pallas_call x1, Pallas kernels, fused(): pl.pallas_call(functools.partial(kernel, depth_z, taps_count), out_shape=...  52.6 us

profile of v2, /device:TPU:1, one launch (start us, length us, event | category | flops | bytes accessed | tf_op | source)
XLA Modules:
  0.0 53.4 jit_solution(636530965734068143)
XLA Ops:
  0.0 52.6 %shard_map.73 = bf16[128,2048]{1,0:T(8,128)(2,1)S(1)} custom-call(bf16[128,2048]{1,0:T(8,128)(2,1)} %bitcast.8, bf16[64,1024]{1,0:T(8,128)(2,1)} %bitcast.9, bf16[64,1024]{1,0:T(8,128)(2,1)} %bitcast.10, bf16[512,128]{1,0:T(8,128)(2,1)} %wo_hbm.1, bf16[31,1024]{1,0:T(8,128)(2,1)} %bitcast.11, f32[1,1024]{1,0:T(1,128)} %bitcast.12, f32[1,1024]{1,0:T(1,128)} %bitcast.13), custom_call_target="tpu_custom_call" | custom-call | tf_op jit(solution)/shard_map/pallas_call | solution.py:329
  52.6 0.8 %copy.9 = bf16[1,128,2048]{2,1,0:T(8,128)(2,1)} copy(bf16[1,128,2048]{2,1,0:T(8,128)(2,1)S(1)} %bitcast.7) | data formatting | bytes 1048576

commit v3 on v2

--- a/solution.py
+++ b/solution.py
@@ -12,10 +12,10 @@
 EDGE = 16
 
 
-def kernel(depth_z, taps_count, tok_hbm, wv_hbm, wg_hbm, wo_hbm, taps_ref, gain_ref, bias_ref, out_ref,
-           tok, wg, wo, gp, cs, call, act, tb,
+def kernel(depth_z, taps_count, tok_hbm, wv_hbm, wg_hbm, wo_hbm, taps_hbm, gain_hbm, bias_hbm, out_ref,
+           tok, wg, wo, gp, cs, call, act, tb, taps_ref, gain_ref, bias_ref,
            load_sem, tok_s, tok_r, w_s, w_r, wd_s, wd_r, halo_s, halo_r,
-           cv_s, cv_r, oz_s, oz_r, op_s, op_r, od_s, od_r):
+           cv_s, cv_r, oz_s, oz_r, dz_s, dz_r, op_s, op_r, od_s, od_r):
     s, c = lax.axis_index("sp"), lax.axis_index("dp")
     q, z = s % GROUP, s // GROUP
     sx = s + 1 - 2 * (s % 2)
@@ -56,6 +56,9 @@
         pltpu.make_async_copy(tok_hbm, tok.at[pl.ds(pl.multiple_of(q * rows, rows), rows), :], load_sem.at[0]),
         pltpu.make_async_copy(wv_hbm, wg_at(c, z).at[0], load_sem.at[1]),
         pltpu.make_async_copy(wg_hbm, wg_at(c, z).at[1], load_sem.at[3]),
+        pltpu.make_async_copy(taps_hbm, taps_ref, load_sem.at[4]),
+        pltpu.make_async_copy(gain_hbm, gain_ref, load_sem.at[5]),
+        pltpu.make_async_copy(bias_hbm, bias_ref, load_sem.at[6]),
         pltpu.make_async_copy(wo_hbm, wo_at(c, z, q), load_sem.at[2]),
     ]
     for load in loads:
@@ -142,6 +145,22 @@
     def own_wo(core, zz):
         return wo_at(core, zz, q)
 
+    def far_wo(core, zz):
+        return wo_at(core, zz, qd)
+
+    def far_line(step):
+        z_recv(far_wo, dz_s, dz_r, step)
+        if step + 1 < steps:
+            z_send(far_wo, dz_s, dz_r, step + 1)
+
+    def sides_finish(at, ss, rs):
+        for kind, who, half, peer in ((0, qx, 0, sx), (2, qy, 1, sy), (1, qx, 1, sx), (3, qy, 0, sy)):
+            remote(at(who, half), at(who, half), ss.at[kind], rs.at[kind], peer, c).wait_recv()
+
+    def sides_sent(at, ss, rs):
+        for kind, half, peer in ((0, 0, sx), (2, 1, sy), (1, 1, sx), (3, 0, sy)):
+            remote(at(q, half), at(q, half), ss.at[kind], rs.at[kind], peer, c).wait_send()
+
     def o_cross(slot):
         index, zz, cond = slot
         return remote(wo_plane(c, zz), wo_plane(c, zz), od_s.at[index], od_r.at[index], s, 1 - c)
@@ -152,7 +171,8 @@
     loads[2].wait()
     z_send(wg_at, w_s, w_r, 0)
     w_cross(slots_by[0])
-    loads[3].wait()
+    for load in loads[3:]:
+        load.wait()
     tiles = depth_z // 2
     lane = lax.broadcasted_iota(jnp.int32, (1, LANES), 1) < LANES // 2
     odd = (q % 2) == 1
@@ -244,7 +264,14 @@
         return carry
 
     o_pass(slots[0])
-    lax.fori_loop(0, tiles * (chunks - 2), inner, 0)
+    half = tiles * (chunks - 2) // 2
+    lax.fori_loop(0, half, inner, 0)
+    for step in range(1, min(2, steps)):
+        o_line(step)
+    square_finish(*o_args(slots[0]))
+    z_send(far_wo, dz_s, dz_r, 0)
+    o_cross(slots[0]).start()
+    lax.fori_loop(half, tiles * (chunks - 2), inner, 0)
     pl.when(z > 0)(lambda: halo_up().wait_recv())
     pl.when(z < steps)(lambda: halo_down().wait_recv())
     lax.fori_loop(0, tiles * 2, outer, 0)
@@ -254,11 +281,9 @@
     for copy in sent:
         copy.start()
     call[q] = cs[q]
-    each(0, o_pass)
-    for step in range(1, steps):
+    for step in range(2, steps):
         o_line(step)
-    square_finish(*o_args(slots[0]))
-    o_cross(slots[0]).start()
+    far_line(0)
     for n, (who, peer) in enumerate(((qd, sd), (qx, sx), (qy, sy))):
         remote(cs.at[who], call.at[who], cv_s.at[n], cv_r.at[n], peer, c).wait_recv()
 
@@ -286,13 +311,13 @@
         out_ref[:, cols] = jnp.dot(act[...], wo[:, cols], preferred_element_type=jnp.float32).astype(jnp.bfloat16)
 
     def gather(slot):
-        square_finish(*o_args(slot))
+        sides_finish(*o_args(slot))
         o_cross(slot).start()
 
     finish(slots[0])
     for step in range(steps):
-        if step + 1 < steps:
-            each(step + 1, o_pass)
+        if step > 0:
+            far_line(step)
         each(step, gather)
         if step > 0:
             each(step - 1, finish)
@@ -302,6 +327,7 @@
     for step in range(steps):
         z_send_wait(wg_at, w_s, w_r, step)
         z_send_wait(own_wo, oz_s, oz_r, step)
+        z_send_wait(far_wo, dz_s, dz_r, step)
     pl.when(z < steps)(lambda: halo_up().wait_send())
     pl.when(z > 0)(lambda: halo_down().wait_send())
     for copy in sent:
@@ -310,7 +336,7 @@
         def drain(slot=slot):
             index, zz, cond = slot
             remote(wg_at(c, zz), wg_at(c, zz), wd_s.at[index], wd_r.at[index], s, 1 - c).wait_send()
-            square_sent(*o_args(slot))
+            (square_sent if index == 0 else sides_sent)(*o_args(slot))
             o_cross(slot).wait_send()
         guarded(slot[2], drain)
 
@@ -329,7 +355,7 @@
     mixed = pl.pallas_call(
         functools.partial(kernel, depth_z, taps_count),
         out_shape=pltpu.VMEM((rows, w_out.shape[1] * GROUP * depth_z), bf16),
-        in_specs=[far, far, far, far, near, near, near],
+        in_specs=[far] * 7,
         out_specs=near,
         scratch_shapes=[
             pltpu.VMEM((span, width), bf16),
@@ -340,9 +366,12 @@
             pltpu.VMEM((GROUP, rows, tiles * LANES), bf16),
             pltpu.VMEM((rows, channels), bf16),
             pltpu.VMEM((tiles, taps_count, 8, LANES), jnp.float32),
-            dma((4,)), dma((6,)), dma((6,)), dma((2, steps)), dma((2, steps)),
+            pltpu.VMEM(conv_taps.shape[::-1], bf16),
+            pltpu.VMEM((1, channels), jnp.float32),
+            pltpu.VMEM((1, channels), jnp.float32),
+            dma((7,)), dma((6,)), dma((6,)), dma((2, steps)), dma((2, steps)),
             dma((slots,)), dma((slots,)), dma((2,)), dma((2,)),
-            dma((3,)), dma((3,)), dma((2, steps)), dma((2, steps)),
+            dma((3,)), dma((3,)), dma((2, steps)), dma((2, steps)), dma((2, steps)), dma((2, steps)),
             dma((slots, 6)), dma((slots, 6)), dma((slots,)), dma((slots,)),
         ],
         compiler_params=pltpu.CompilerParams(collective_id=0, has_side_effects=True),

time: 53.6 us -> 51.9 us (0.968)
  Pallas kernels: 52.6 us -> 51 us
    pallas_call x1, Pallas kernels: 52.6 us -> 51 us  [fused(): pl.pallas_call(functools.partial(kernel, depth_z, taps_count), out_shape=...]
where the time goes in v3:
time: 51.9 us; the launch traced here: 51.8 us
  Pallas kernels  51 us (98%)
  local copies, waits for them, and re-layouts  0.8 us (2%)
    pallas_call x1, Pallas kernels, fused(): pl.pallas_call(functools.partial(kernel, depth_z, taps_count), out_shape=...  51 us

profile of v3, /device:TPU:1, one launch (start us, length us, event | category | flops | bytes accessed | tf_op | source)
XLA Modules:
  0.0 51.8 jit_solution(12824586189262378813)
XLA Ops:
  0.0 51.0 %shard_map.73 = bf16[128,2048]{1,0:T(8,128)(2,1)S(1)} custom-call(bf16[128,2048]{1,0:T(8,128)(2,1)} %bitcast.8, bf16[64,1024]{1,0:T(8,128)(2,1)} %bitcast.9, bf16[64,1024]{1,0:T(8,128)(2,1)} %bitcast.10, bf16[512,128]{1,0:T(8,128)(2,1)} %wo_hbm.1, bf16[31,1024]{1,0:T(8,128)(2,1)} %bitcast.11, f32[1,1024]{1,0:T(1,128)} %bitcast.12, f32[1,1024]{1,0:T(1,128)} %bitcast.13), custom_call_target="tpu_custom_call" | custom-call | tf_op jit(solution)/shard_map/pallas_call | solution.py:355
  51.0 0.8 %copy.9 = bf16[1,128,2048]{2,1,0:T(8,128)(2,1)} copy(bf16[1,128,2048]{2,1,0:T(8,128)(2,1)S(1)} %bitcast.7) | data formatting | bytes 1048576
